TPU v7x, 32 devices: a whole 2x2x4 slice. The times are simulated.
32 devices in a mesh: sp: 8 (over z, x), tp: 4 (over y, core).
Axes of the slice: x: 2, y: 2, z: 4, core: 2. Of those that a mesh axis runs over, the one named last changes fastest.
Arguments:
- in_gate: bfloat16 [1024, 2048], P('tp', 'sp'), may hold values from -6 to 6
- out_gate: bfloat16 [1024, 2048], P('tp', 'sp'), may hold values from -6 to 6
- values: bfloat16 [1024, 2048], P('tp', 'sp'), may hold values from -6 to 6
- conv_taps: bfloat16 [3, 1024], P(None, 'tp'), may hold values from -3.5 to 3.5
- doc_ids: int32 [2048], P('sp'), may hold values from 0 to 1, as said below
- residual: bfloat16 [2048, 2048], P('sp'), may hold values from -6 to 6
- out_weight: bfloat16 [1024, 2048], P('tp'), may hold values from -0.1875 to 0.1875
- norm_gain: bfloat16 [2048], replicated, may hold values from 0.099609375 to 1.8984375
- routes: int32 [2048, 2], P('sp'), may hold values from 0 to 7, all different within a row; in each aligned block of 256 rows (0 to 255, 256 to 511, ...) at most 96 rows name the same one
- route_weights: float32 [2048, 2], P('sp'), may hold values from 0.2 to 1
- expert_gate: bfloat16 [8, 2048, 4224], P('sp', None, 'tp'), may hold values from -0.125 to 0.125
- expert_up: bfloat16 [8, 2048, 4224], P('sp', None, 'tp'), may hold values from -0.125 to 0.125
- expert_down: bfloat16 [8, 4224, 2048], P('sp', 'tp'), may hold values from -0.09375 to 0.09375
Outputs:
- merged: bfloat16 [2048, 2048], P('sp', 'tp')
Inputs may be any that keep to these rules, and one draw needn't show every extreme that they name: `routes`: each row names 2 different experts. Within the rows of one index of sp (aligned blocks of 256 rows) no expert is named more than 96 times, a bound that some expert reaches in some blocks. `doc_ids`: never falls along the sequence; starts at 0 and rises by one at each of 1 document starts, each number used.
All inputs are finite; a program needn't handle non-finite values.
Results may differ from a plain program's by a relative error of at most 0.019.
Values may be sent and summed in bfloat16 or wider, within the bound.
A program may use at most 64 MiB of HBM per device.

v0:
```python
import functools

import jax
import jax.numpy as jnp
from jax import lax
from jax.experimental import pallas as pl
from jax.experimental.pallas import tpu as pltpu
from jax.sharding import PartitionSpec as P

EPSILON = 1e-06


def shifted(x, axis, by):
    count = lax.axis_size(axis)
    pairs = [(i, i + by) for i in range(count) if 0 <= i + by < count]
    return lax.ppermute(x, axis, pairs)


def shards(
    in_gate,
    out_gate,
    values,
    conv_taps,
    doc_ids,
    residual,
    out_weight,
    norm_gain,
    routes,
    route_weights,
    expert_gate,
    expert_up,
    expert_down,
):
    gated_in = (in_gate.astype(jnp.float32) * values.astype(jnp.float32)).astype(jnp.bfloat16)
    tail_rows, tail_docs = shifted((gated_in[:, -2:], doc_ids[-2:]), "sp", 1)
    extended = lax.optimization_barrier(jnp.concatenate([tail_rows, gated_in], axis=1)).astype(
        jnp.float32
    )
    docs_ext = jnp.concatenate([tail_docs, doc_ids])
    length = doc_ids.shape[0]
    near_mask = (docs_ext[1 : length + 1] == doc_ids).astype(jnp.float32)
    far_mask = (docs_ext[0:length] == doc_ids).astype(jnp.float32)
    tap_values = conv_taps.astype(jnp.float32)
    convolved = (
        tap_values[2][:, None] * extended[:, 2:]
        + tap_values[1][:, None] * extended[:, 1 : length + 1] * near_mask[None, :]
        + tap_values[0][:, None] * extended[:, 0:length] * far_mask[None, :]
    )
    mixed_rows = (out_gate.astype(jnp.float32) * convolved).astype(jnp.bfloat16)
    partial_value = lax.dot_general(
        mixed_rows, out_weight, (((0,), (0,)), ((), ())), preferred_element_type=jnp.float32
    )
    tp_count = lax.axis_size("tp")
    model_width = residual.shape[1]
    share_width = model_width // tp_count
    column = lax.axis_index("tp") * share_width
    stream = residual.astype(jnp.float32) + lax.psum(
        partial_value.astype(jnp.bfloat16), "tp"
    ).astype(jnp.float32)
    inv_rms = lax.rsqrt(jnp.mean(stream * stream, axis=1, keepdims=True) + EPSILON)
    normed = (stream * inv_rms * norm_gain.astype(jnp.float32)[None, :]).astype(jnp.bfloat16)
    stream_cols = lax.dynamic_slice_in_dim(stream, column, share_width, 1)
    own_cols = lax.dynamic_slice_in_dim(normed, column, share_width, 1)
    tokens = routes.shape[0]
    top_count = routes.shape[1]
    experts = lax.axis_size("sp")
    capacity = 3 * tokens * top_count // (2 * experts)
    chosen = routes.reshape(-1)
    hits_table = (chosen[:, None] == jnp.arange(experts, dtype=jnp.int32)[None, :]).astype(
        jnp.int32
    )
    earlier = jnp.cumsum(hits_table, axis=0) - hits_table
    ranked = jnp.sum(earlier * hits_table, axis=1)
    slot_index = chosen * capacity + ranked
    owners = jnp.arange(tokens * top_count, dtype=jnp.int32) // top_count
    source = jnp.zeros((experts * capacity,), jnp.int32).at[slot_index].set(owners)
    filled = jnp.zeros((experts * capacity,), jnp.bool_).at[slot_index].set(True)
    gate_weight = expert_gate[0]
    up_weight = expert_up[0]
    down_weight = expert_down[0]
    picked = jnp.where(
        filled[:, None], jnp.take(own_cols, source, axis=0), jnp.zeros((), jnp.bfloat16)
    ).reshape(experts, capacity, share_width)
    arrived = lax.all_to_all(picked, "sp", split_axis=0, concat_axis=0, tiled=True)
    slot_count = arrived.shape[1]
    row_block = arrived.reshape(-1, share_width)
    piece_cols = lax.all_gather(row_block, "tp", axis=1, tiled=True)
    gate_sum = jnp.dot(piece_cols, gate_weight, preferred_element_type=jnp.float32)
    up_sum = jnp.dot(piece_cols, up_weight, preferred_element_type=jnp.float32)
    hidden = (jax.nn.silu(gate_sum) * up_sum).astype(jnp.bfloat16)
    down_sum = jnp.dot(hidden, down_weight, preferred_element_type=jnp.float32)
    summed = lax.psum_scatter(down_sum.astype(jnp.bfloat16), "tp", scatter_dimension=1, tiled=True)
    returned = lax.all_to_all(
        summed.reshape(experts, slot_count, share_width),
        "sp",
        split_axis=0,
        concat_axis=0,
        tiled=True,
    )
    results = jnp.take(returned.reshape(experts * capacity, share_width), slot_index, axis=0)
    results = results.astype(jnp.float32).reshape(tokens, top_count, share_width)
    blended = jnp.sum(route_weights[:, :, None] * results, axis=1)
    return (stream_cols + blended).astype(jnp.bfloat16)

MESH = pl.DeviceIdType.MESH
F32 = jnp.float32
BF16 = jnp.bfloat16
LANES = 128


def xor_index(value, mask):
    bit = 1
    while bit <= mask:
        if mask & bit:
            value = value + bit - 2 * bit * lax.rem(lax.div(value, bit), 2)
        bit *= 2
    return value


def column_of(row, width):
    return jnp.transpose(jnp.broadcast_to(row, (LANES, row.shape[1])))[:, :width]


def across_rows(left, right):
    return lax.dot_general(left, right, (((1,), (1,)), ((), ())), preferred_element_type=F32)


def plan_groups(planes):
    near, far = range(1, planes // 2), range(planes // 2, planes) if planes > 1 else ()
    groups = [(0, (0, 1))]
    groups += [(mask, (0, 1)) for mask in range(1, planes)]
    return groups


def layer_kernel(
    sp_count,
    capacity,
    in_gate_ref,
    out_gate_ref,
    values_ref,
    taps_ref,
    docs_ref,
    residual_ref,
    out_weight_ref,
    gain_ref,
    routes_ref,
    weights_ref,
    gate_hbm,
    up_hbm,
    down_hbm,
    out_ref,
    gate_ref,
    up_ref,
    down_ref,
    gains,
    own_residual,
    gated,
    halo,
    halo_docs,
    share,
    share_in,
    pair_sum,
    pair_in,
    edge,
    edge_in,
    squares,
    squares_in,
    keys,
    select,
    weight_cols,
    stream,
    picked,
    rows_ref,
    down_share,
    down_in,
    down_pair,
    down_pair_in,
    finished,
    back,
    halo_send,
    halo_recv,
    local_sem,
    share_send,
    share_recv,
    pair_send,
    pair_recv,
    edge_send,
    edge_recv,
    square_send,
    square_recv,
    row_send,
    row_recv,
    spread_send,
    spread_recv,
    half_send,
    half_recv,
    cross_send,
    cross_recv,
    back_send,
    back_recv,
):
    me = lax.axis_index("sp")
    rank = lax.axis_index("tp")
    side, core = lax.div(rank, 2), lax.rem(rank, 2)
    plane, lane = lax.div(me, 2), lax.rem(me, 2)
    partner = 2 * side + 1 - core
    across = 2 * (1 - side) + core
    diagonal = 2 * (1 - side) + 1 - core
    channels, tokens = in_gate_ref.shape
    model_width = residual_ref.shape[1]
    width = stream.shape[1]
    groups = plan_groups(sp_count // 2)
    stages = len(groups)

    def cols(owner):
        return pl.ds(pl.multiple_of(owner * width, width), width)

    def remote(src, dst, send, recv, device):
        return pltpu.make_async_remote_copy(
            src_ref=src, dst_ref=dst, send_sem=send, recv_sem=recv, device_id=device, device_id_type=MESH
        )

    local = [
        pltpu.make_async_copy(residual_ref.at[:, cols(rank)], own_residual, local_sem.at[0]),
        pltpu.make_async_copy(gate_hbm.at[0], gate_ref, local_sem.at[1]),
        pltpu.make_async_copy(up_hbm.at[0], up_ref, local_sem.at[2]),
        pltpu.make_async_copy(down_hbm.at[0], down_ref, local_sem.at[3]),
    ]
    for copy in local:
        copy.start()

    barrier = pltpu.get_barrier_semaphore()
    for step in range(1, sp_count):
        pl.semaphore_signal(
            barrier, inc=1, device_id={"sp": lax.rem(me + step, sp_count)}, device_id_type=MESH
        )
    for other in (partner, across, diagonal):
        pl.semaphore_signal(barrier, inc=1, device_id={"tp": other}, device_id_type=MESH)

    gains[...] = gain_ref[...].astype(F32)
    gated[...] = (in_gate_ref[...].astype(F32) * values_ref[...].astype(F32)).astype(BF16)
    taps = [column_of(taps_ref[k : k + 1, :].astype(F32), LANES) for k in range(3)]
    wide_taps = [jnp.concatenate([tap] * (tokens // LANES), axis=1) for tap in taps]
    docs = jnp.broadcast_to(docs_ref[...], (8, tokens))
    token_row = lax.broadcasted_iota(jnp.int32, (8, tokens), 1)

    def same_document(by):
        alike = (pltpu.roll(docs, by, 1) == docs) & (token_row >= by)
        return jnp.where(alike, 1.0, 0.0)[0:1, :]

    main = gated[...].astype(F32)
    convolved = (
        wide_taps[2] * main
        + wide_taps[1] * pltpu.roll(main, 1, 1) * same_document(1)
        + wide_taps[0] * pltpu.roll(main, 2, 1) * same_document(2)
    )
    mixed = jnp.transpose(out_gate_ref[...].astype(F32) * convolved).astype(BF16)

    def projected(owner):
        return jnp.dot(mixed, out_weight_ref[:, cols(owner)], preferred_element_type=F32)

    to_partner = [
        remote(
            share.at[k], share_in.at[k], share_send.at[k], share_recv.at[k], {"tp": partner}
        )
        for k in range(2)
    ]
    share[0] = projected(diagonal).astype(BF16)
    pl.semaphore_wait(barrier, sp_count + 2)
    to_partner[0].start()
    following = lax.rem(me + 1, sp_count)
    tail = gated.at[:, pl.ds(tokens - LANES, LANES)]
    halo_copies = [
        remote(tail, halo, halo_send.at[0], halo_recv.at[0], {"sp": following}),
        remote(docs_ref, halo_docs, halo_send.at[1], halo_recv.at[1], {"sp": following}),
    ]
    for copy in halo_copies:
        copy.start()
    share[1] = projected(partner).astype(BF16)
    to_partner[1].start()
    crossing = projected(across)
    stream[...] = projected(rank)
    to_partner[0].wait_recv()
    pair_sum[...] = (crossing + share_in[0].astype(F32)).astype(BF16)
    pair_copy = remote(pair_sum, pair_in, pair_send.at[0], pair_recv.at[0], {"tp": across})
    pair_copy.start()

    for copy in halo_copies:
        copy.wait_recv()
    earlier = jnp.where(me > 0, halo[...].astype(F32), 0.0)
    extended = jnp.concatenate([earlier, jnp.zeros_like(earlier)], axis=1)
    old_docs = jnp.broadcast_to(halo_docs[...], (8, tokens))[:, tokens - LANES :]
    docs_ext = jnp.concatenate([old_docs, docs[:, :LANES]], axis=1)
    near = jnp.where(pltpu.roll(docs_ext, 1, 1)[:, LANES:] == docs[:, :LANES], 1.0, 0.0)[0:1, :]
    far = jnp.where(pltpu.roll(docs_ext, 2, 1)[:, LANES:] == docs[:, :LANES], 1.0, 0.0)[0:1, :]
    carried = (
        taps[1] * pltpu.roll(extended, 1, 1)[:, LANES:] * near
        + taps[0] * pltpu.roll(extended, 2, 1)[:, LANES:] * far
    )
    head_rows = edge.shape[1]
    edge_mixed = jnp.transpose(out_gate_ref[:, 0:LANES].astype(F32) * carried)[0:head_rows, :]
    edge_mixed = edge_mixed.astype(BF16)

    def edge_projected(owner):
        return jnp.dot(edge_mixed, out_weight_ref[:, cols(owner)], preferred_element_type=F32)

    edge_copies = []
    for k, other in enumerate((partner, across, diagonal)):
        edge[k] = edge_projected(other).astype(BF16)
        copy = remote(edge.at[k], edge_in.at[k], edge_send.at[k], edge_recv.at[k], {"tp": other})
        copy.start()
        edge_copies.append(copy)
    stream[0:head_rows, :] += edge_projected(rank)
    to_partner[1].wait_recv()
    local[0].wait()
    stream[...] += share_in[1].astype(F32) + own_residual[...].astype(F32)

    experts = lax.broadcasted_iota(jnp.int32, (sp_count, tokens), 0)
    hits = jnp.zeros((sp_count, tokens), F32)
    expert_weights = jnp.zeros((sp_count, tokens), F32)
    for k in range(routes_ref.shape[0]):
        named = routes_ref[k : k + 1, :] == experts
        hits = jnp.where(named, 1.0, hits)
        expert_weights = jnp.where(named, weights_ref[k : k + 1, :], expert_weights)
    before = lax.broadcasted_iota(jnp.int32, (tokens, tokens), 0) < lax.broadcasted_iota(
        jnp.int32, (tokens, tokens), 1
    )
    ranks = jnp.dot(
        hits.astype(BF16), jnp.where(before, 1.0, 0.0).astype(BF16), preferred_element_type=F32
    )
    key_rows = jnp.where(hits > 0.5, ranks, -1.0)
    keys[...] = key_rows
    slots = lax.broadcasted_iota(jnp.int32, (tokens, LANES), 1).astype(F32)
    for expert_index in range(sp_count):
        one = slice(expert_index, expert_index + 1)
        chosen = column_of(key_rows[one, :], LANES) == slots
        select[expert_index] = jnp.where(chosen, 1.0, 0.0).astype(BF16)[:, :capacity]
        weight_cols[expert_index] = column_of(expert_weights[one, :], LANES)

    for copy in edge_copies:
        copy.wait_recv()
    stream[0:head_rows, :] += (
        edge_in[0].astype(F32) + edge_in[1].astype(F32) + edge_in[2].astype(F32)
    )
    pair_copy.wait_recv()
    total = stream[...] + pair_in[...].astype(F32)
    stream[...] = total

    own_square = jnp.sum(total * total, axis=1, keepdims=True)
    squares[...] = jnp.transpose(jnp.broadcast_to(own_square, (tokens, LANES)))[0:8, :]
    square_copies = [
        remote(
            squares, squares_in.at[k], square_send.at[k], square_recv.at[k], {"tp": other}
        )
        for k, other in enumerate((partner, across, diagonal))
    ]
    for copy in square_copies:
        copy.start()
    for copy in square_copies:
        copy.wait_recv()
    all_squares = squares[...] + squares_in[0] + squares_in[1] + squares_in[2]
    inv_rms = column_of(lax.rsqrt(all_squares / model_width + EPSILON)[0:1, :], LANES)[:, 0:1]
    per_rank = width // LANES
    gain = jnp.concatenate(
        [gains[pl.ds(rank * per_rank + k, 1), :] for k in range(per_rank)], axis=1
    )
    normed = (stream[...] * inv_rms * gain).astype(BF16)

    def sources(stage):
        mask, places = groups[stage]
        pair = 2 * xor_index(plane, mask)
        return [pair + (lane if place == 0 else 1 - lane) for place in places]

    def others(stage):
        return sources(stage)[1 if stage == 0 else 0 :]

    def group_rows(stage):
        return pl.ds(0, capacity * len(groups[stage][1]))

    def block_rows(source):
        return pl.ds(pl.multiple_of(source * capacity, capacity), capacity)

    slot_rows = lax.broadcasted_iota(jnp.int32, (capacity, tokens), 0).astype(F32)

    def pick(target):
        chosen = jnp.where(keys[pl.ds(target, 1), :] == slot_rows, 1.0, 0.0).astype(BF16)
        return jnp.dot(chosen, normed, preferred_element_type=F32).astype(BF16)

    def row_copy(source, target):
        return remote(
            picked.at[target],
            rows_ref.at[block_rows(source), cols(rank)],
            row_send.at[target],
            row_recv.at[source],
            {"sp": target},
        )

    def spread(source, kind):
        owner, device = ((rank, across), (rank, partner), (across, partner))[kind]
        block = rows_ref.at[block_rows(source), cols(owner)]
        return remote(
            block, block, spread_send.at[source, kind], spread_recv.at[source, kind], {"tp": device}
        )

    def spread_arrival(source, kind):
        owner = (across, partner, diagonal)[kind]
        block = rows_ref.at[block_rows(source), cols(owner)]
        return remote(
            block, block, spread_send.at[source, kind], spread_recv.at[source, kind], {"tp": partner}
        )

    rows_ref[block_rows(me), cols(rank)] = pick(me)
    spread(me, 0).start()
    spread(me, 1).start()
    for stage in range(stages):
        for target in others(stage):
            picked[target] = pick(target)
            row_copy(me, target).start()

    def direct(stage):
        for source in others(stage):
            block = rows_ref.at[block_rows(source), cols(rank)]
            remote(
                block, block, row_send.at[source], row_recv.at[source], {"sp": source}
            ).wait_recv()
            spread(source, 0).start()
            spread(source, 1).start()

    def relay(stage):
        for source in sources(stage):
            spread_arrival(source, 0).wait_recv()
            spread(source, 2).start()

    def half_copy(stage, k):
        return remote(
            down_share.at[stage, k, group_rows(stage)],
            down_in.at[stage, k, group_rows(stage)],
            half_send.at[stage, k],
            half_recv.at[stage, k],
            {"tp": partner},
        )

    def expert(stage):
        for source in sources(stage):
            spread_arrival(source, 1).wait_recv()
            spread_arrival(source, 2).wait_recv()
        mask, places = groups[stage]
        count = capacity * len(places)
        source = sources(stage)[0] if len(places) == 1 else 2 * xor_index(plane, mask)
        block = rows_ref[pl.ds(pl.multiple_of(source * capacity, count), count), :]
        gate_sum = across_rows(gate_ref[...], block)
        up_sum = across_rows(up_ref[...], block)
        hidden = jnp.transpose(gate_sum / (1.0 + jnp.exp(-gate_sum)) * up_sum).astype(BF16)
        for k, owner in enumerate((diagonal, partner, across, rank)):
            down_share[stage, k, group_rows(stage)] = jnp.dot(
                hidden, down_ref[:, cols(owner)], preferred_element_type=F32
            ).astype(BF16)
            if k < 2:
                half_copy(stage, k).start()

    def cross_copy(stage):
        return remote(
            down_pair.at[stage, group_rows(stage)],
            down_pair_in.at[stage, group_rows(stage)],
            cross_send.at[stage],
            cross_recv.at[stage],
            {"tp": across},
        )

    def cross(stage):
        half_copy(stage, 0).wait_recv()
        rows = group_rows(stage)
        down_pair[stage, rows] = (
            down_share[stage, 2, rows].astype(F32) + down_in[stage, 0, rows].astype(F32)
        ).astype(BF16)
        cross_copy(stage).start()

    def part_rows(stage, source):
        if len(groups[stage][1]) == 1:
            return pl.ds(0, capacity)
        return pl.ds(pl.multiple_of(lax.rem(source, 2) * capacity, capacity), capacity)

    def back_copy(stage, source):
        return remote(
            finished.at[stage, part_rows(stage, source)],
            back.at[me],
            back_send.at[source],
            back_recv.at[me],
            {"sp": source},
        )

    def finish(stage):
        half_copy(stage, 1).wait_recv()
        cross_copy(stage).wait_recv()
        rows = group_rows(stage)
        finished[stage, rows] = (
            down_share[stage, 3, rows].astype(F32)
            + down_in[stage, 1, rows].astype(F32)
            + down_pair_in[stage, rows].astype(F32)
        ).astype(BF16)
        for source in others(stage):
            back_copy(stage, source).start()

    def each(action, stage):
        if 0 <= stage < stages:
            action(stage)

    for stage in range(1):
        each(direct, stage)
    for stage in range(stages + 3):
        each(direct, stage + 1)
        each(relay, stage)
        each(cross, stage - 1)
        if stage == 0:
            for copy in local[1:]:
                copy.wait()
        each(expert, stage)
        each(finish, stage - 2)

    def add_result(source, block):
        weight = weight_cols[source][:, 0:1]
        stream[...] += weight * jnp.dot(select[source], block, preferred_element_type=F32)

    for stage in range(stages):
        for place, source in enumerate(sources(stage)):
            if stage == 0 and place == 0:
                add_result(source, finished[stage, part_rows(stage, source)])
            else:
                remote(
                    back.at[source],
                    back.at[source],
                    back_send.at[source],
                    back_recv.at[source],
                    {"sp": source},
                ).wait_recv()
                add_result(source, back[source])
    out_ref[...] = stream[...].astype(BF16)

    for copy in halo_copies + to_partner + [pair_copy] + edge_copies + square_copies:
        copy.wait_send()
    for stage in range(stages):
        for place, source in enumerate(sources(stage)):
            if stage > 0 or place > 0:
                row_copy(me, source).wait_send()
                back_copy(stage, source).wait_send()
            for kind in range(3):
                spread(source, kind).wait_send()
        half_copy(stage, 0).wait_send()
        half_copy(stage, 1).wait_send()
        cross_copy(stage).wait_send()


def fused(
    sp_count,
    in_gate,
    out_gate,
    values,
    conv_taps,
    doc_ids,
    residual,
    out_weight,
    norm_gain,
    routes,
    route_weights,
    expert_gate,
    expert_up,
    expert_down,
):
    channels, tokens = in_gate.shape
    model_width = residual.shape[1]
    width = model_width // 4
    capacity = 3 * tokens * routes.shape[1] // (2 * sp_count)
    hidden = expert_gate.shape[2]
    stages = len(plan_groups(sp_count // 2))
    pair_rows = 2 * capacity
    vmem = pl.BlockSpec(memory_space=pltpu.VMEM)
    hbm = pl.BlockSpec(memory_space=pl.ANY)
    dma = pltpu.SemaphoreType.DMA
    return pl.pallas_call(
        functools.partial(layer_kernel, sp_count, capacity),
        out_shape=jax.ShapeDtypeStruct((tokens, width), BF16),
        in_specs=[vmem] * 5 + [hbm] + [vmem] * 4 + [hbm] * 3,
        out_specs=vmem,
        scratch_shapes=[
            pltpu.VMEM((hidden, model_width), BF16),
            pltpu.VMEM((hidden, model_width), BF16),
            pltpu.VMEM((hidden, model_width), BF16),
            pltpu.VMEM((model_width // LANES, LANES), F32),
            pltpu.VMEM((tokens, width), BF16),
            pltpu.VMEM((channels, tokens), BF16),
            pltpu.VMEM((channels, LANES), BF16),
            pltpu.VMEM((1, tokens), jnp.int32),
            pltpu.VMEM((2, tokens, width), BF16),
            pltpu.VMEM((2, tokens, width), BF16),
            pltpu.VMEM((tokens, width), BF16),
            pltpu.VMEM((tokens, width), BF16),
            pltpu.VMEM((3, 16, width), BF16),
            pltpu.VMEM((3, 16, width), BF16),
            pltpu.VMEM((8, tokens), F32),
            pltpu.VMEM((3, 8, tokens), F32),
            pltpu.VMEM((sp_count, tokens), F32),
            pltpu.VMEM((sp_count, tokens, capacity), BF16),
            pltpu.VMEM((sp_count, tokens, LANES), F32),
            pltpu.VMEM((tokens, width), F32),
            pltpu.VMEM((sp_count, capacity, width), BF16),
            pltpu.VMEM((sp_count * capacity, model_width), BF16),
            pltpu.VMEM((stages, 4, pair_rows, width), BF16),
            pltpu.VMEM((stages, 2, pair_rows, width), BF16),
            pltpu.VMEM((stages, pair_rows, width), BF16),
            pltpu.VMEM((stages, pair_rows, width), BF16),
            pltpu.VMEM((stages, pair_rows, width), BF16),
            pltpu.VMEM((sp_count, capacity, width), BF16),
            dma((2,)),
            dma((2,)),
            dma((4,)),
            dma((2,)),
            dma((2,)),
            dma((1,)),
            dma((1,)),
            dma((3,)),
            dma((3,)),
            dma((3,)),
            dma((3,)),
            dma((sp_count,)),
            dma((sp_count,)),
            dma((sp_count, 3)),
            dma((sp_count, 3)),
            dma((stages, 2)),
            dma((stages, 2)),
            dma((stages,)),
            dma((stages,)),
            dma((sp_count,)),
            dma((sp_count,)),
        ],
        compiler_params=pltpu.CompilerParams(
            collective_id=0, has_side_effects=True, vmem_limit_bytes=60 * 1024 * 1024
        ),
    )(
        in_gate,
        out_gate,
        values,
        conv_taps,
        doc_ids.reshape(1, tokens),
        residual,
        out_weight,
        norm_gain.reshape(model_width // LANES, LANES),
        routes.T,
        route_weights.T,
        expert_gate.transpose(0, 2, 1),
        expert_up.transpose(0, 2, 1),
        expert_down,
    )


def solution(mesh):
    placed = (
        P("tp", "sp"),
        P("tp", "sp"),
        P("tp", "sp"),
        P(None, "tp"),
        P("sp"),
        P("sp", None),
        P("tp", None),
        P(),
        P("sp", None),
        P("sp", None),
        P("sp", None, "tp"),
        P("sp", None, "tp"),
        P("sp", "tp", None),
    )
    sp_count, tp_count = mesh.shape["sp"], mesh.shape["tp"]
    planes = sp_count // 2
    paired = tp_count == 4 and sp_count % 2 == 0 and planes & (planes - 1) == 0
    body = functools.partial(fused, sp_count) if paired else shards
    return jax.shard_map(
        body, mesh=mesh, in_specs=placed, out_specs=P("sp", "tp"), check_vma=False
    )
```

profile of v0, /device:TPU:13, one launch (start us, length us, event | category | flops | bytes accessed | tf_op | source)
XLA Modules:
  0.0 77.4 jit_solution(4144695309308172738)
XLA Ops:
  0.0 75.7 %shard_map.127 = bf16[256,512]{1,0:T(8,128)(2,1)} custom-call(bf16[256,256]{1,0:T(8,128)(2,1)} %in_gate_ref.1, bf16[256,256]{1,0:T(8,128)(2,1)} %out_gate_ref.1, bf16[256,256]{1,0:T(8,128)(2,1)} %values_ref.1, bf16[3,256]{1,0:T(4,128)(2,1)} %taps_ref.1, s32[1,256]{1,0:T(1,128)} %bitcast.11, bf16[256,2048]{1,0:T(8,128)(2,1)} %residual_ref.1, ...), custom_call_target="tpu_custom_call" | custom-call | tf_op jit(solution)/shard_map/pallas_call | solution.py:579
  75.7 1.7 %copy.15 = bf16[256,512]{1,0:T(8,128)(2,1)} copy(bf16[256,512]{1,0:T(8,128)(2,1)} %shard_map.127) | data formatting | bytes 524288
where the time goes:
time: 77.5 us; the launch traced here: 77.4 us
  Pallas kernels  75.7 us (98%)
  local copies, waits for them, and re-layouts  1.67 us (2%)
    pallas_call x1, Pallas kernels, fused(): pl.pallas_call(functools.partial(layer_kernel, sp_count, capacity), out_s...  75.7 us
    unnamed x1, local copies, waits for them, and re-layouts  1.67 us

commit v1 on v0

--- a/solution.py
+++ b/solution.py
@@ -125,11 +125,10 @@
     return lax.dot_general(left, right, (((1,), (1,)), ((), ())), preferred_element_type=F32)
 
 
-def plan_groups(planes):
-    near, far = range(1, planes // 2), range(planes // 2, planes) if planes > 1 else ()
-    groups = [(0, (0, 1))]
-    groups += [(mask, (0, 1)) for mask in range(1, planes)]
-    return groups
+def plan_stages(planes):
+    far = [(mask, flip) for mask in range(planes // 2, planes) for flip in (0, 1)]
+    near = [(0, 1)] + [(mask, flip) for mask in range(1, planes // 2) for flip in (0, 1)] + [(0, 0)]
+    return list(zip(far, near))
 
 
 def layer_kernel(
@@ -155,6 +154,7 @@
     gains,
     own_residual,
     gated,
+    tail,
     halo,
     halo_docs,
     share,
@@ -168,9 +168,13 @@
     keys,
     select,
     weight_cols,
+    scales,
+    scales_in,
     stream,
     picked,
     rows_ref,
+    gate_part,
+    up_part,
     down_share,
     down_in,
     down_pair,
@@ -188,6 +192,8 @@
     edge_recv,
     square_send,
     square_recv,
+    scale_send,
+    scale_recv,
     row_send,
     row_recv,
     spread_send,
@@ -209,16 +215,25 @@
     channels, tokens = in_gate_ref.shape
     model_width = residual_ref.shape[1]
     width = stream.shape[1]
-    groups = plan_groups(sp_count // 2)
-    stages = len(groups)
+    half_width = width // 2
+    places = plan_stages(sp_count // 2)
+    stages = len(places)
+    own = (stages - 1, 1)
 
     def cols(owner):
         return pl.ds(pl.multiple_of(owner * width, width), width)
+
+    def chip_cols(which):
+        return pl.ds(pl.multiple_of(which * 2 * width, 2 * width), 2 * width)
 
     def remote(src, dst, send, recv, device):
         return pltpu.make_async_remote_copy(
             src_ref=src, dst_ref=dst, send_sem=send, recv_sem=recv, device_id=device, device_id_type=MESH
         )
+
+    def peer(at):
+        mask, flip = places[at[0]][at[1]]
+        return 2 * xor_index(plane, mask) + (1 - lane if flip else lane)
 
     local = [
         pltpu.make_async_copy(residual_ref.at[:, cols(rank)], own_residual, local_sem.at[0]),
@@ -239,8 +254,14 @@
 
     gains[...] = gain_ref[...].astype(F32)
     gated[...] = (in_gate_ref[...].astype(F32) * values_ref[...].astype(F32)).astype(BF16)
-    taps = [column_of(taps_ref[k : k + 1, :].astype(F32), LANES) for k in range(3)]
-    wide_taps = [jnp.concatenate([tap] * (tokens // LANES), axis=1) for tap in taps]
+    head_rows = tail.shape[0]
+    tail[...] = jnp.transpose(gated[:, tokens - LANES :].astype(F32))[LANES - head_rows :, :].astype(
+        BF16
+    )
+    tap_rows = [taps_ref[k : k + 1, :].astype(F32) for k in range(3)]
+    wide_taps = [
+        jnp.concatenate([column_of(tap, LANES)] * (tokens // LANES), axis=1) for tap in tap_rows
+    ]
     docs = jnp.broadcast_to(docs_ref[...], (8, tokens))
     token_row = lax.broadcasted_iota(jnp.int32, (8, tokens), 1)
 
@@ -259,59 +280,82 @@
     def projected(owner):
         return jnp.dot(mixed, out_weight_ref[:, cols(owner)], preferred_element_type=F32)
 
+    halves = [pl.ds(k * half_width, half_width) for k in range(2)]
     to_partner = [
         remote(
-            share.at[k], share_in.at[k], share_send.at[k], share_recv.at[k], {"tp": partner}
+            share.at[0, :, halves[k]],
+            share_in.at[0, :, halves[k]],
+            share_send.at[k],
+            share_recv.at[k],
+            {"tp": partner},
         )
         for k in range(2)
-    ]
+    ] + [remote(share.at[1], share_in.at[1], share_send.at[2], share_recv.at[2], {"tp": partner})]
     share[0] = projected(diagonal).astype(BF16)
-    pl.semaphore_wait(barrier, sp_count + 2)
-    to_partner[0].start()
     following = lax.rem(me + 1, sp_count)
-    tail = gated.at[:, pl.ds(tokens - LANES, LANES)]
     halo_copies = [
         remote(tail, halo, halo_send.at[0], halo_recv.at[0], {"sp": following}),
         remote(docs_ref, halo_docs, halo_send.at[1], halo_recv.at[1], {"sp": following}),
     ]
+    pair_copies = [
+        remote(
+            pair_sum.at[:, halves[k]],
+            pair_in.at[:, halves[k]],
+            pair_send.at[k],
+            pair_recv.at[k],
+            {"tp": across},
+        )
+        for k in range(2)
+    ]
+
+    def send_pair(k):
+        to_partner[k].wait_recv()
+        pair_sum[:, halves[k]] = (
+            crossing[:, k * half_width : (k + 1) * half_width]
+            + share_in[0, :, halves[k]].astype(F32)
+        ).astype(BF16)
+        pair_copies[k].start()
+
+    pl.semaphore_wait(barrier, sp_count + 2)
+    to_partner[0].start()
+    to_partner[1].start()
     for copy in halo_copies:
         copy.start()
+    crossing = projected(across)
+    send_pair(0)
     share[1] = projected(partner).astype(BF16)
-    to_partner[1].start()
-    crossing = projected(across)
+    to_partner[2].start()
     stream[...] = projected(rank)
-    to_partner[0].wait_recv()
-    pair_sum[...] = (crossing + share_in[0].astype(F32)).astype(BF16)
-    pair_copy = remote(pair_sum, pair_in, pair_send.at[0], pair_recv.at[0], {"tp": across})
-    pair_copy.start()
 
     for copy in halo_copies:
         copy.wait_recv()
     earlier = jnp.where(me > 0, halo[...].astype(F32), 0.0)
-    extended = jnp.concatenate([earlier, jnp.zeros_like(earlier)], axis=1)
     old_docs = jnp.broadcast_to(halo_docs[...], (8, tokens))[:, tokens - LANES :]
     docs_ext = jnp.concatenate([old_docs, docs[:, :LANES]], axis=1)
-    near = jnp.where(pltpu.roll(docs_ext, 1, 1)[:, LANES:] == docs[:, :LANES], 1.0, 0.0)[0:1, :]
-    far = jnp.where(pltpu.roll(docs_ext, 2, 1)[:, LANES:] == docs[:, :LANES], 1.0, 0.0)[0:1, :]
-    carried = (
-        taps[1] * pltpu.roll(extended, 1, 1)[:, LANES:] * near
-        + taps[0] * pltpu.roll(extended, 2, 1)[:, LANES:] * far
-    )
-    head_rows = edge.shape[1]
-    edge_mixed = jnp.transpose(out_gate_ref[:, 0:LANES].astype(F32) * carried)[0:head_rows, :]
+
+    def carried_mask(by):
+        alike = pltpu.roll(docs_ext, by, 1)[:, LANES:] == docs[:, :LANES]
+        alike = alike & (token_row[:, :LANES] < by)
+        return column_of(jnp.where(alike, 1.0, 0.0)[0:1, :], LANES)[0:head_rows, 0:1]
+
+    carried = tap_rows[1] * pltpu.roll(earlier, 1, 0) * carried_mask(1) + tap_rows[0] * pltpu.roll(
+        earlier, 2, 0
+    ) * carried_mask(2)
+    edge_mixed = jnp.transpose(out_gate_ref[:, 0:LANES].astype(F32))[0:head_rows, :] * carried
     edge_mixed = edge_mixed.astype(BF16)
 
     def edge_projected(owner):
         return jnp.dot(edge_mixed, out_weight_ref[:, cols(owner)], preferred_element_type=F32)
 
     edge_copies = []
-    for k, other in enumerate((partner, across, diagonal)):
+    for k, other in enumerate((across, diagonal, partner)):
         edge[k] = edge_projected(other).astype(BF16)
         copy = remote(edge.at[k], edge_in.at[k], edge_send.at[k], edge_recv.at[k], {"tp": other})
         copy.start()
         edge_copies.append(copy)
+    send_pair(1)
     stream[0:head_rows, :] += edge_projected(rank)
-    to_partner[1].wait_recv()
+    to_partner[2].wait_recv()
     local[0].wait()
     stream[...] += share_in[1].astype(F32) + own_residual[...].astype(F32)
 
@@ -330,21 +374,88 @@
     )
     key_rows = jnp.where(hits > 0.5, ranks, -1.0)
     keys[...] = key_rows
-    slots = lax.broadcasted_iota(jnp.int32, (tokens, LANES), 1).astype(F32)
+    slot_lanes = select.shape[2]
+    lanes = lax.broadcasted_iota(jnp.int32, (tokens, slot_lanes), 1)
+    slots = jnp.where(lanes < capacity, lanes, lanes - capacity)
+    slots = jnp.where(lanes < 2 * capacity, slots, -2).astype(F32)
     for expert_index in range(sp_count):
         one = slice(expert_index, expert_index + 1)
-        chosen = column_of(key_rows[one, :], LANES) == slots
-        select[expert_index] = jnp.where(chosen, 1.0, 0.0).astype(BF16)[:, :capacity]
+        key_cols = jnp.concatenate(
+            [column_of(key_rows[one, :], LANES)] * (slot_lanes // LANES), axis=1
+        )
+        select[expert_index] = jnp.where(key_cols == slots, 1.0, 0.0).astype(BF16)
         weight_cols[expert_index] = column_of(expert_weights[one, :], LANES)
 
+    per_rank = width // LANES
+    gain = jnp.concatenate(
+        [gains[pl.ds(rank * per_rank + k, 1), :] for k in range(per_rank)], axis=1
+    )
     for copy in edge_copies:
         copy.wait_recv()
     stream[0:head_rows, :] += (
         edge_in[0].astype(F32) + edge_in[1].astype(F32) + edge_in[2].astype(F32)
     )
-    pair_copy.wait_recv()
+    for copy in pair_copies:
+        copy.wait_recv()
     total = stream[...] + pair_in[...].astype(F32)
     stream[...] = total
+    scaled = (total * gain).astype(BF16)
+
+    def place_rows(at):
+        return pl.ds(at[1] * capacity, capacity)
+
+    slot_rows = lax.broadcasted_iota(jnp.int32, (capacity, tokens), 0).astype(F32)
+
+    def index(at):
+        return 2 * at[0] + at[1]
+
+    def pick(at):
+        chosen = jnp.where(keys[pl.ds(peer(at), 1), :] == slot_rows, 1.0, 0.0).astype(BF16)
+        return jnp.dot(chosen, scaled, preferred_element_type=F32).astype(BF16)
+
+    def own_block(at):
+        return rows_ref.at[at[0], place_rows(at), cols(rank)]
+
+    def row_copy(at):
+        return remote(
+            picked.at[index(at)],
+            own_block(at),
+            row_send.at[index(at)],
+            row_recv.at[index(at)],
+            {"sp": peer(at)},
+        )
+
+    def spread(at, kind):
+        owner, device = ((rank, across), (rank, partner), (across, partner))[kind]
+        block = rows_ref.at[at[0], place_rows(at), cols(owner)]
+        p = index(at)
+        return remote(
+            block, block, spread_send.at[p, kind], spread_recv.at[p, kind], {"tp": device}
+        )
+
+    def spread_arrival(at, kind):
+        owner = (across, partner, diagonal)[kind]
+        block = rows_ref.at[at[0], place_rows(at), cols(owner)]
+        p = index(at)
+        return remote(
+            block, block, spread_send.at[p, kind], spread_recv.at[p, kind], {"tp": partner}
+        )
+
+    def send_rows(at):
+        if at == own:
+            rows_ref[at[0], place_rows(at), cols(rank)] = pick(at)
+            spread(at, 0).start()
+            spread(at, 1).start()
+        else:
+            picked[index(at)] = pick(at)
+            row_copy(at).start()
+
+    everyone = [(stage, place) for stage in range(stages) for place in range(2)]
+    send_order = [(0, 0), (0, 1), own] + [
+        at for stage in range(1, stages) for at in ((stage, 1), (stage, 0)) if at != own
+    ]
+    for at in send_order:
+        send_rows(at)
 
     own_square = jnp.sum(total * total, axis=1, keepdims=True)
     squares[...] = jnp.transpose(jnp.broadcast_to(own_square, (tokens, LANES)))[0:8, :]
@@ -359,195 +470,179 @@
     for copy in square_copies:
         copy.wait_recv()
     all_squares = squares[...] + squares_in[0] + squares_in[1] + squares_in[2]
-    inv_rms = column_of(lax.rsqrt(all_squares / model_width + EPSILON)[0:1, :], LANES)[:, 0:1]
-    per_rank = width // LANES
-    gain = jnp.concatenate(
-        [gains[pl.ds(rank * per_rank + k, 1), :] for k in range(per_rank)], axis=1
-    )
-    normed = (stream[...] * inv_rms * gain).astype(BF16)
-
-    def sources(stage):
-        mask, places = groups[stage]
-        pair = 2 * xor_index(plane, mask)
-        return [pair + (lane if place == 0 else 1 - lane) for place in places]
-
-    def others(stage):
-        return sources(stage)[1 if stage == 0 else 0 :]
-
-    def group_rows(stage):
-        return pl.ds(0, capacity * len(groups[stage][1]))
-
-    def block_rows(source):
-        return pl.ds(pl.multiple_of(source * capacity, capacity), capacity)
-
-    slot_rows = lax.broadcasted_iota(jnp.int32, (capacity, tokens), 0).astype(F32)
-
-    def pick(target):
-        chosen = jnp.where(keys[pl.ds(target, 1), :] == slot_rows, 1.0, 0.0).astype(BF16)
-        return jnp.dot(chosen, normed, preferred_element_type=F32).astype(BF16)
-
-    def row_copy(source, target):
+    inv_rms = column_of(lax.rsqrt(all_squares / model_width + EPSILON)[0:1, :], LANES)
+    inv_cols = jnp.concatenate([inv_rms] * (slot_lanes // LANES), axis=1)
+
+    def scale_copy(at):
+        p = index(at)
         return remote(
-            picked.at[target],
-            rows_ref.at[block_rows(source), cols(rank)],
-            row_send.at[target],
-            row_recv.at[source],
-            {"sp": target},
-        )
-
-    def spread(source, kind):
-        owner, device = ((rank, across), (rank, partner), (across, partner))[kind]
-        block = rows_ref.at[block_rows(source), cols(owner)]
-        return remote(
-            block, block, spread_send.at[source, kind], spread_recv.at[source, kind], {"tp": device}
-        )
-
-    def spread_arrival(source, kind):
-        owner = (across, partner, diagonal)[kind]
-        block = rows_ref.at[block_rows(source), cols(owner)]
-        return remote(
-            block, block, spread_send.at[source, kind], spread_recv.at[source, kind], {"tp": partner}
-        )
-
-    rows_ref[block_rows(me), cols(rank)] = pick(me)
-    spread(me, 0).start()
-    spread(me, 1).start()
-    for stage in range(stages):
-        for target in others(stage):
-            picked[target] = pick(target)
-            row_copy(me, target).start()
-
-    def direct(stage):
-        for source in others(stage):
-            block = rows_ref.at[block_rows(source), cols(rank)]
-            remote(
-                block, block, row_send.at[source], row_recv.at[source], {"sp": source}
-            ).wait_recv()
-            spread(source, 0).start()
-            spread(source, 1).start()
-
-    def relay(stage):
-        for source in sources(stage):
-            spread_arrival(source, 0).wait_recv()
-            spread(source, 2).start()
+            scales.at[p], scales_in.at[p], scale_send.at[p], scale_recv.at[p], {"sp": peer(at)}
+        )
+
+    for at in send_order:
+        row = jnp.sum(select[peer(at)].astype(F32) * inv_cols, axis=0, keepdims=True)
+        if at == own:
+            scales_in[index(at)] = jnp.broadcast_to(row, scales.shape[1:])
+        else:
+            scales[index(at)] = jnp.broadcast_to(row, scales.shape[1:])
+            scale_copy(at).start()
+
+    def direct(at):
+        row_copy(at).wait_recv()
+        spread(at, 0).start()
+        spread(at, 1).start()
+
+    def relay(at):
+        spread_arrival(at, 0).wait_recv()
+        spread(at, 2).start()
 
     def half_copy(stage, k):
         return remote(
-            down_share.at[stage, k, group_rows(stage)],
-            down_in.at[stage, k, group_rows(stage)],
+            down_share.at[stage, k],
+            down_in.at[stage, k],
             half_send.at[stage, k],
             half_recv.at[stage, k],
             {"tp": partner},
         )
 
-    def expert(stage):
-        for source in sources(stage):
-            spread_arrival(source, 1).wait_recv()
-            spread_arrival(source, 2).wait_recv()
-        mask, places = groups[stage]
-        count = capacity * len(places)
-        source = sources(stage)[0] if len(places) == 1 else 2 * xor_index(plane, mask)
-        block = rows_ref[pl.ds(pl.multiple_of(source * capacity, count), count), :]
-        gate_sum = across_rows(gate_ref[...], block)
-        up_sum = across_rows(up_ref[...], block)
+    def expert_near(stage):
+        for place in range(2):
+            spread_arrival((stage, place), 1).wait_recv()
+        block = rows_ref[stage, :, chip_cols(side)]
+        gate_part[stage % 2] = across_rows(gate_ref[:, chip_cols(side)], block)
+        up_part[stage % 2] = across_rows(up_ref[:, chip_cols(side)], block)
+
+    def expert_far(stage):
+        for place in range(2):
+            spread_arrival((stage, place), 2).wait_recv()
+            if (stage, place) != own:
+                scale_copy((stage, place)).wait_recv()
+        block = rows_ref[stage, :, chip_cols(1 - side)]
+        scale_lane = lax.broadcasted_iota(jnp.int32, scales.shape[1:], 1)
+        scale = jnp.where(scale_lane < capacity, scales_in[2 * stage], scales_in[2 * stage + 1])
+        scale = scale[0:1, 0 : 2 * capacity]
+        gate_sum = gate_part[stage % 2] + across_rows(gate_ref[:, chip_cols(1 - side)], block)
+        up_sum = up_part[stage % 2] + across_rows(up_ref[:, chip_cols(1 - side)], block)
+        gate_sum = gate_sum * scale
+        up_sum = up_sum * scale
         hidden = jnp.transpose(gate_sum / (1.0 + jnp.exp(-gate_sum)) * up_sum).astype(BF16)
         for k, owner in enumerate((diagonal, partner, across, rank)):
-            down_share[stage, k, group_rows(stage)] = jnp.dot(
+            down_share[stage, k] = jnp.dot(
                 hidden, down_ref[:, cols(owner)], preferred_element_type=F32
             ).astype(BF16)
             if k < 2:
                 half_copy(stage, k).start()
 
-    def cross_copy(stage):
+    def cross_copy(at):
         return remote(
-            down_pair.at[stage, group_rows(stage)],
-            down_pair_in.at[stage, group_rows(stage)],
-            cross_send.at[stage],
-            cross_recv.at[stage],
+            down_pair.at[at[0], place_rows(at)],
+            down_pair_in.at[at[0], place_rows(at)],
+            cross_send.at[index(at)],
+            cross_recv.at[index(at)],
             {"tp": across},
         )
 
-    def cross(stage):
-        half_copy(stage, 0).wait_recv()
-        rows = group_rows(stage)
+    def cross(at):
+        stage, rows = at[0], place_rows(at)
+        if at[1] == 0:
+            half_copy(stage, 0).wait_recv()
         down_pair[stage, rows] = (
             down_share[stage, 2, rows].astype(F32) + down_in[stage, 0, rows].astype(F32)
         ).astype(BF16)
-        cross_copy(stage).start()
-
-    def part_rows(stage, source):
-        if len(groups[stage][1]) == 1:
-            return pl.ds(0, capacity)
-        return pl.ds(pl.multiple_of(lax.rem(source, 2) * capacity, capacity), capacity)
-
-    def back_copy(stage, source):
+        cross_copy(at).start()
+
+    def back_copy(at):
+        p = index(at)
         return remote(
-            finished.at[stage, part_rows(stage, source)],
-            back.at[me],
-            back_send.at[source],
-            back_recv.at[me],
-            {"sp": source},
-        )
-
-    def finish(stage):
-        half_copy(stage, 1).wait_recv()
-        cross_copy(stage).wait_recv()
-        rows = group_rows(stage)
+            finished.at[at[0], place_rows(at)],
+            back.at[p],
+            back_send.at[p],
+            back_recv.at[p],
+            {"sp": peer(at)},
+        )
+
+    def finish(at):
+        stage, rows = at[0], place_rows(at)
+        if at[1] == 0:
+            half_copy(stage, 1).wait_recv()
+        cross_copy(at).wait_recv()
         finished[stage, rows] = (
             down_share[stage, 3, rows].astype(F32)
             + down_in[stage, 1, rows].astype(F32)
             + down_pair_in[stage, rows].astype(F32)
         ).astype(BF16)
-        for source in others(stage):
-            back_copy(stage, source).start()
-
-    def each(action, stage):
+        if at != own:
+            back_copy(at).start()
+
+    def add_result(at):
+        source = peer(at)
+        if at == own:
+            block = finished[at[0], place_rows(at)]
+        else:
+            back_copy(at).wait_recv()
+            block = back[index(at)]
+        weight = weight_cols[source][:, 0:1]
+        stream[...] += weight * jnp.dot(
+            select[source][:, 0:capacity], block, preferred_element_type=F32
+        )
+
+    def each(action, stage, place):
         if 0 <= stage < stages:
-            action(stage)
-
-    for stage in range(1):
-        each(direct, stage)
-    for stage in range(stages + 3):
-        each(direct, stage + 1)
-        each(relay, stage)
-        each(cross, stage - 1)
-        if stage == 0:
-            for copy in local[1:]:
-                copy.wait()
-        each(expert, stage)
-        each(finish, stage - 2)
-
-    def add_result(source, block):
-        weight = weight_cols[source][:, 0:1]
-        stream[...] += weight * jnp.dot(select[source], block, preferred_element_type=F32)
-
+            action((stage, place))
+
+    def each_remote(action, stage, place):
+        if (stage, place) != own:
+            each(action, stage, place)
+
+    each_remote(direct, 0, 1)
+    relay(own)
+    direct((0, 0))
+    each_remote(direct, 1, 1)
+    for copy in local[1:]:
+        copy.wait()
     for stage in range(stages):
-        for place, source in enumerate(sources(stage)):
-            if stage == 0 and place == 0:
-                add_result(source, finished[stage, part_rows(stage, source)])
-            else:
-                remote(
-                    back.at[source],
-                    back.at[source],
-                    back_send.at[source],
-                    back_recv.at[source],
-                    {"sp": source},
-                ).wait_recv()
-                add_result(source, back[source])
+        each_remote(relay, stage, 1)
+        if stage == stages - 1:
+            for early in range(stages - 2):
+                cross((early, 1))
+        expert_near(stage)
+        relay((stage, 0))
+        each(direct, stage + 1, 0)
+        each(cross, stage - 1, 0)
+        each_remote(direct, stage + 2, 1)
+        each(finish, stage - 2, 0)
+        expert_far(stage)
+    for stage in range(stages - 2):
+        finish((stage, 1))
+    cross((stages - 1, 0))
+    finish((stages - 2, 0))
+    cross((stages - 2, 1))
+    cross(own)
+    add_result((0, 0))
+    finish((stages - 1, 0))
+    add_result((0, 1))
+    finish((stages - 2, 1))
+    for stage in range(1, stages - 1):
+        add_result((stage, 0))
+        add_result((stage, 1))
+    finish(own)
+    add_result(own)
+    add_result((stages - 1, 0))
     out_ref[...] = stream[...].astype(BF16)
 
-    for copy in halo_copies + to_partner + [pair_copy] + edge_copies + square_copies:
+    for copy in halo_copies + to_partner + pair_copies + edge_copies + square_copies:
         copy.wait_send()
+    for at in everyone:
+        if at != own:
+            row_copy(at).wait_send()
+            scale_copy(at).wait_send()
+            back_copy(at).wait_send()
+        for kind in range(3):
+            spread(at, kind).wait_send()
+        cross_copy(at).wait_send()
     for stage in range(stages):
-        for place, source in enumerate(sources(stage)):
-            if stage > 0 or place > 0:
-                row_copy(me, source).wait_send()
-                back_copy(stage, source).wait_send()
-            for kind in range(3):
-                spread(source, kind).wait_send()
         half_copy(stage, 0).wait_send()
         half_copy(stage, 1).wait_send()
-        cross_copy(stage).wait_send()
 
 
 def fused(
@@ -570,8 +665,9 @@
     model_width = residual.shape[1]
     width = model_width // 4
     capacity = 3 * tokens * routes.shape[1] // (2 * sp_count)
+    slot_lanes = -(-2 * capacity // LANES) * LANES
     hidden = expert_gate.shape[2]
-    stages = len(plan_groups(sp_count // 2))
+    stages = len(plan_stages(sp_count // 2))
     pair_rows = 2 * capacity
     vmem = pl.BlockSpec(memory_space=pltpu.VMEM)
     hbm = pl.BlockSpec(memory_space=pl.ANY)
@@ -588,7 +684,8 @@
             pltpu.VMEM((model_width // LANES, LANES), F32),
             pltpu.VMEM((tokens, width), BF16),
             pltpu.VMEM((channels, tokens), BF16),
-            pltpu.VMEM((channels, LANES), BF16),
+            pltpu.VMEM((16, channels), BF16),
+            pltpu.VMEM((16, channels), BF16),
             pltpu.VMEM((1, tokens), jnp.int32),
             pltpu.VMEM((2, tokens, width), BF16),
             pltpu.VMEM((2, tokens, width), BF16),
@@ -599,11 +696,15 @@
             pltpu.VMEM((8, tokens), F32),
             pltpu.VMEM((3, 8, tokens), F32),
             pltpu.VMEM((sp_count, tokens), F32),
-            pltpu.VMEM((sp_count, tokens, capacity), BF16),
+            pltpu.VMEM((sp_count, tokens, slot_lanes), BF16),
             pltpu.VMEM((sp_count, tokens, LANES), F32),
+            pltpu.VMEM((sp_count, 8, slot_lanes), F32),
+            pltpu.VMEM((sp_count, 8, slot_lanes), F32),
             pltpu.VMEM((tokens, width), F32),
             pltpu.VMEM((sp_count, capacity, width), BF16),
-            pltpu.VMEM((sp_count * capacity, model_width), BF16),
+            pltpu.VMEM((stages, pair_rows, model_width), BF16),
+            pltpu.VMEM((2, hidden, pair_rows), F32),
+            pltpu.VMEM((2, hidden, pair_rows), F32),
             pltpu.VMEM((stages, 4, pair_rows, width), BF16),
             pltpu.VMEM((stages, 2, pair_rows, width), BF16),
             pltpu.VMEM((stages, pair_rows, width), BF16),
@@ -613,22 +714,24 @@
             dma((2,)),
             dma((2,)),
             dma((4,)),
+            dma((3,)),
+            dma((3,)),
             dma((2,)),
             dma((2,)),
-            dma((1,)),
-            dma((1,)),
             dma((3,)),
             dma((3,)),
             dma((3,)),
             dma((3,)),
             dma((sp_count,)),
             dma((sp_count,)),
+            dma((sp_count,)),
+            dma((sp_count,)),
             dma((sp_count, 3)),
             dma((sp_count, 3)),
             dma((stages, 2)),
             dma((stages, 2)),
-            dma((stages,)),
-            dma((stages,)),
+            dma((sp_count,)),
+            dma((sp_count,)),
             dma((sp_count,)),
             dma((sp_count,)),
         ],
@@ -670,7 +773,7 @@
     )
     sp_count, tp_count = mesh.shape["sp"], mesh.shape["tp"]
     planes = sp_count // 2
-    paired = tp_count == 4 and sp_count % 2 == 0 and planes & (planes - 1) == 0
+    paired = tp_count == 4 and sp_count % 4 == 0 and planes & (planes - 1) == 0
     body = functools.partial(fused, sp_count) if paired else shards
     return jax.shard_map(
         body, mesh=mesh, in_specs=placed, out_specs=P("sp", "tp"), check_vma=False

time: 77.5 us -> 71.4 us (0.921)
  the two profiles are of different devices: /device:TPU:13 before, /device:TPU:0 now
where the time goes in v1:
time: 71.4 us; the launch traced here: 71.3 us
  Pallas kernels  69.6 us (97%)
  local copies, waits for them, and re-layouts  1.67 us (2%)
    pallas_call x1, Pallas kernels, fused(): pl.pallas_call(functools.partial(layer_kernel, sp_count, capacity), out_s...  69.6 us
    unnamed x1, local copies, waits for them, and re-layouts  1.67 us

profile of v1, /device:TPU:0, one launch (start us, length us, event | category | flops | bytes accessed | tf_op | source)
XLA Modules:
  0.0 71.3 jit_solution(3190017990043676417)
XLA Ops:
  0.0 69.6 %shard_map.127 = bf16[256,512]{1,0:T(8,128)(2,1)} custom-call(bf16[256,256]{1,0:T(8,128)(2,1)} %in_gate_ref.1, bf16[256,256]{1,0:T(8,128)(2,1)} %out_gate_ref.1, bf16[256,256]{1,0:T(8,128)(2,1)} %values_ref.1, bf16[3,256]{1,0:T(4,128)(2,1)} %taps_ref.1, s32[1,256]{1,0:T(1,128)} %bitcast.11, bf16[256,2048]{1,0:T(8,128)(2,1)} %residual_ref.1, ...), custom_call_target="tpu_custom_call" | custom-call | tf_op jit(solution)/shard_map/pallas_call | solution.py:675
  69.6 1.7 %copy.15 = bf16[256,512]{1,0:T(8,128)(2,1)} copy(bf16[256,512]{1,0:T(8,128)(2,1)} %shard_map.127) | data formatting | bytes 524288

commit v2 on v1

--- a/solution.py
+++ b/solution.py
@@ -129,6 +129,38 @@
     far = [(mask, flip) for mask in range(planes // 2, planes) for flip in (0, 1)]
     near = [(0, 1)] + [(mask, flip) for mask in range(1, planes // 2) for flip in (0, 1)] + [(0, 0)]
     return list(zip(far, near))
+
+
+FOUR_STAGE_ORDER = (
+    "S10 S21 D01 D11",
+    "L31 D00 S20 W",
+    "N0 L01 D10 N1",
+    "S30 L11 D21 L00",
+    "G0 L10 D20 Q0",
+    "R0 X00 G1 L21",
+    "Q1 R1 D30 X10",
+    "N2 L20 X01 N3",
+    "F00 G2 L30 Q2",
+    "R2 X20 X21 F10",
+    "G3 Q3 R3 F01",
+    "X30 X11 X31 F20",
+    "A00 F21 F30 F11",
+    "A10 A01 F31 A31",
+    "A20 A21 E A11",
+    "A30",
+)
+
+
+def plan_order(stages):
+    if stages == 4:
+        return " ".join(FOUR_STAGE_ORDER).split()
+    blocks = [f"{stage}{place}" for stage in range(stages) for place in range(2)]
+    order = ["S" + block for block in blocks[2:-1] if block != "11"]
+    order += ["D" + block for block in blocks[:-1]] + ["L" + block for block in blocks] + ["W"]
+    for stage in range(stages):
+        order += [f"{step}{stage}" for step in "NGQR"]
+        order += [f"X{stage}0", f"X{stage}1", f"F{stage}0", f"F{stage}1"]
+    return order + ["E"] + ["A" + block for block in blocks]
 
 
 def layer_kernel(
@@ -175,6 +207,7 @@
     rows_ref,
     gate_part,
     up_part,
+    hidden_ref,
     down_share,
     down_in,
     down_pair,
@@ -297,23 +330,26 @@
         remote(tail, halo, halo_send.at[0], halo_recv.at[0], {"sp": following}),
         remote(docs_ref, halo_docs, halo_send.at[1], halo_recv.at[1], {"sp": following}),
     ]
+    middle = tokens // 2
+    pair_parts = [
+        (slice(0, 1), slice(head_rows, tokens)),
+        (slice(1, 2), slice(middle, tokens)),
+        (slice(0, 2), slice(0, head_rows)),
+        (slice(1, 2), slice(head_rows, middle)),
+    ]
     pair_copies = [
-        remote(
-            pair_sum.at[:, halves[k]],
-            pair_in.at[:, halves[k]],
-            pair_send.at[k],
-            pair_recv.at[k],
-            {"tp": across},
-        )
-        for k in range(2)
+        remote(pair_sum.at[at], pair_in.at[at], pair_send.at[k], pair_recv.at[k], {"tp": across})
+        for k, at in enumerate(pair_parts)
     ]
 
-    def send_pair(k):
-        to_partner[k].wait_recv()
-        pair_sum[:, halves[k]] = (
-            crossing[:, k * half_width : (k + 1) * half_width]
-            + share_in[0, :, halves[k]].astype(F32)
-        ).astype(BF16)
+    def send_pair(k, extra=None):
+        which, rows = pair_parts[k]
+        for h in range(which.start, which.stop):
+            columns = slice(h * half_width, (h + 1) * half_width)
+            block = crossing[rows, columns] + share_in[0, rows, columns].astype(F32)
+            if extra is not None:
+                block = block + extra[:, columns]
+            pair_sum[h, rows] = block.astype(BF16)
         pair_copies[k].start()
 
     pl.semaphore_wait(barrier, sp_count + 2)
@@ -322,7 +358,10 @@
     for copy in halo_copies:
         copy.start()
     crossing = projected(across)
+    to_partner[0].wait_recv()
     send_pair(0)
+    to_partner[1].wait_recv()
+    send_pair(1)
     share[1] = projected(partner).astype(BF16)
     to_partner[2].start()
     stream[...] = projected(rank)
@@ -347,13 +386,17 @@
     def edge_projected(owner):
         return jnp.dot(edge_mixed, out_weight_ref[:, cols(owner)], preferred_element_type=F32)
 
-    edge_copies = []
-    for k, other in enumerate((across, diagonal, partner)):
-        edge[k] = edge_projected(other).astype(BF16)
-        copy = remote(edge.at[k], edge_in.at[k], edge_send.at[k], edge_recv.at[k], {"tp": other})
-        copy.start()
-        edge_copies.append(copy)
-    send_pair(1)
+    edge_copies = [
+        remote(edge.at[k], edge_in.at[k], edge_send.at[k], edge_recv.at[k], {"tp": partner})
+        for k in range(2)
+    ]
+    for k, owner in enumerate((diagonal, partner)):
+        edge[k] = edge_projected(owner).astype(BF16)
+        edge_copies[k].start()
+    crossing_edge = edge_projected(across)
+    edge_copies[0].wait_recv()
+    send_pair(2, crossing_edge + edge_in[0].astype(F32))
+    send_pair(3)
     stream[0:head_rows, :] += edge_projected(rank)
     to_partner[2].wait_recv()
     local[0].wait()
@@ -390,16 +433,16 @@
     gain = jnp.concatenate(
         [gains[pl.ds(rank * per_rank + k, 1), :] for k in range(per_rank)], axis=1
     )
-    for copy in edge_copies:
-        copy.wait_recv()
-    stream[0:head_rows, :] += (
-        edge_in[0].astype(F32) + edge_in[1].astype(F32) + edge_in[2].astype(F32)
-    )
-    for copy in pair_copies:
-        copy.wait_recv()
-    total = stream[...] + pair_in[...].astype(F32)
-    stream[...] = total
-    scaled = (total * gain).astype(BF16)
+    edge_copies[1].wait_recv()
+    stream[0:head_rows, :] += edge_in[1].astype(F32)
+
+    def scaled_half(k):
+        for part in ((0, 2), (1, 3))[k]:
+            pair_copies[part].wait_recv()
+        total = stream[:, halves[k]] + pair_in[k].astype(F32)
+        stream[:, halves[k]] = total
+        own_gain = gain[:, k * half_width : (k + 1) * half_width]
+        return (total * own_gain).astype(BF16), jnp.sum(total * total, axis=1, keepdims=True)
 
     def place_rows(at):
         return pl.ds(at[1] * capacity, capacity)
@@ -409,25 +452,23 @@
     def index(at):
         return 2 * at[0] + at[1]
 
-    def pick(at):
+    def pick(at, k):
         chosen = jnp.where(keys[pl.ds(peer(at), 1), :] == slot_rows, 1.0, 0.0).astype(BF16)
-        return jnp.dot(chosen, scaled, preferred_element_type=F32).astype(BF16)
-
-    def own_block(at):
-        return rows_ref.at[at[0], place_rows(at), cols(rank)]
-
-    def row_copy(at):
+        return jnp.dot(chosen, scaled[k], preferred_element_type=F32).astype(BF16)
+
+    def row_copy(at, k):
+        p = index(at)
         return remote(
-            picked.at[index(at)],
-            own_block(at),
-            row_send.at[index(at)],
-            row_recv.at[index(at)],
+            picked.at[p, k],
+            rows_ref.at[at[0], rank, k, place_rows(at)],
+            row_send.at[p, k],
+            row_recv.at[p, k],
             {"sp": peer(at)},
         )
 
     def spread(at, kind):
         owner, device = ((rank, across), (rank, partner), (across, partner))[kind]
-        block = rows_ref.at[at[0], place_rows(at), cols(owner)]
+        block = rows_ref.at[at[0], owner, :, place_rows(at)]
         p = index(at)
         return remote(
             block, block, spread_send.at[p, kind], spread_recv.at[p, kind], {"tp": device}
@@ -435,29 +476,38 @@
 
     def spread_arrival(at, kind):
         owner = (across, partner, diagonal)[kind]
-        block = rows_ref.at[at[0], place_rows(at), cols(owner)]
+        block = rows_ref.at[at[0], owner, :, place_rows(at)]
         p = index(at)
         return remote(
             block, block, spread_send.at[p, kind], spread_recv.at[p, kind], {"tp": partner}
         )
 
-    def send_rows(at):
+    def fill_rows(at, k):
         if at == own:
-            rows_ref[at[0], place_rows(at), cols(rank)] = pick(at)
-            spread(at, 0).start()
-            spread(at, 1).start()
+            rows_ref[at[0], rank, k, place_rows(at)] = pick(at, k)
         else:
-            picked[index(at)] = pick(at)
-            row_copy(at).start()
+            picked[index(at), k] = pick(at, k)
+
+    def send_rows(at, k):
+        if at != own:
+            row_copy(at, k).start()
 
     everyone = [(stage, place) for stage in range(stages) for place in range(2)]
-    send_order = [(0, 0), (0, 1), own] + [
+    send_order = [(0, 1), own, (0, 0)] + [
         at for stage in range(1, stages) for at in ((stage, 1), (stage, 0)) if at != own
     ]
-    for at in send_order:
-        send_rows(at)
-
-    own_square = jnp.sum(total * total, axis=1, keepdims=True)
+    first = send_order[:4]
+    scaled, half_squares = [], []
+    for k in range(2):
+        block, square = scaled_half(k)
+        scaled.append(block)
+        half_squares.append(square)
+        if k == 0:
+            for at in first:
+                fill_rows(at, k)
+                send_rows(at, k)
+
+    own_square = half_squares[0] + half_squares[1]
     squares[...] = jnp.transpose(jnp.broadcast_to(own_square, (tokens, LANES)))[0:8, :]
     square_copies = [
         remote(
@@ -467,11 +517,12 @@
     ]
     for copy in square_copies:
         copy.start()
-    for copy in square_copies:
-        copy.wait_recv()
-    all_squares = squares[...] + squares_in[0] + squares_in[1] + squares_in[2]
-    inv_rms = column_of(lax.rsqrt(all_squares / model_width + EPSILON)[0:1, :], LANES)
-    inv_cols = jnp.concatenate([inv_rms] * (slot_lanes // LANES), axis=1)
+    for at in first:
+        fill_rows(at, 1)
+        send_rows(at, 1)
+        if at == own:
+            spread(at, 0).start()
+            spread(at, 1).start()
 
     def scale_copy(at):
         p = index(at)
@@ -479,16 +530,23 @@
             scales.at[p], scales_in.at[p], scale_send.at[p], scale_recv.at[p], {"sp": peer(at)}
         )
 
-    for at in send_order:
-        row = jnp.sum(select[peer(at)].astype(F32) * inv_cols, axis=0, keepdims=True)
-        if at == own:
-            scales_in[index(at)] = jnp.broadcast_to(row, scales.shape[1:])
-        else:
-            scales[index(at)] = jnp.broadcast_to(row, scales.shape[1:])
-            scale_copy(at).start()
+    def send_scales():
+        for copy in square_copies:
+            copy.wait_recv()
+        all_squares = squares[...] + squares_in[0] + squares_in[1] + squares_in[2]
+        inv_rms = column_of(lax.rsqrt(all_squares / model_width + EPSILON)[0:1, :], LANES)
+        inv_cols = jnp.concatenate([inv_rms] * (slot_lanes // LANES), axis=1)
+        for at in send_order:
+            row = jnp.sum(select[peer(at)].astype(F32) * inv_cols, axis=0, keepdims=True)
+            if at == own:
+                scales_in[index(at)] = jnp.broadcast_to(row, scales.shape[1:])
+            else:
+                scales[index(at)] = jnp.broadcast_to(row, scales.shape[1:])
+                scale_copy(at).start()
 
     def direct(at):
-        row_copy(at).wait_recv()
+        row_copy(at, 0).wait_recv()
+        row_copy(at, 1).wait_recv()
         spread(at, 0).start()
         spread(at, 1).start()
 
@@ -505,10 +563,21 @@
             {"tp": partner},
         )
 
+    arrived = set()
+
+    def half_arrival(stage, k):
+        if (stage, k) not in arrived:
+            arrived.add((stage, k))
+            half_copy(stage, k).wait_recv()
+
+    def chip_rows(stage, which):
+        pieces = [rows_ref[stage, 2 * which + k // 2, k % 2] for k in range(4)]
+        return jnp.concatenate(pieces, axis=1)
+
     def expert_near(stage):
         for place in range(2):
             spread_arrival((stage, place), 1).wait_recv()
-        block = rows_ref[stage, :, chip_cols(side)]
+        block = chip_rows(stage, side)
         gate_part[stage % 2] = across_rows(gate_ref[:, chip_cols(side)], block)
         up_part[stage % 2] = across_rows(up_ref[:, chip_cols(side)], block)
 
@@ -517,7 +586,7 @@
             spread_arrival((stage, place), 2).wait_recv()
             if (stage, place) != own:
                 scale_copy((stage, place)).wait_recv()
-        block = rows_ref[stage, :, chip_cols(1 - side)]
+        block = chip_rows(stage, 1 - side)
         scale_lane = lax.broadcasted_iota(jnp.int32, scales.shape[1:], 1)
         scale = jnp.where(scale_lane < capacity, scales_in[2 * stage], scales_in[2 * stage + 1])
         scale = scale[0:1, 0 : 2 * capacity]
@@ -525,13 +594,16 @@
         up_sum = up_part[stage % 2] + across_rows(up_ref[:, chip_cols(1 - side)], block)
         gate_sum = gate_sum * scale
         up_sum = up_sum * scale
-        hidden = jnp.transpose(gate_sum / (1.0 + jnp.exp(-gate_sum)) * up_sum).astype(BF16)
-        for k, owner in enumerate((diagonal, partner, across, rank)):
-            down_share[stage, k] = jnp.dot(
-                hidden, down_ref[:, cols(owner)], preferred_element_type=F32
-            ).astype(BF16)
-            if k < 2:
-                half_copy(stage, k).start()
+        hidden = gate_sum / (1.0 + jnp.exp(-gate_sum)) * up_sum
+        hidden_ref[stage % 2] = jnp.transpose(hidden).astype(BF16)
+
+    def expert_down(stage, k):
+        owner = (diagonal, partner, across, rank)[k]
+        down_share[stage, k] = jnp.dot(
+            hidden_ref[stage % 2], down_ref[:, cols(owner)], preferred_element_type=F32
+        ).astype(BF16)
+        if k < 2:
+            half_copy(stage, k).start()
 
     def cross_copy(at):
         return remote(
@@ -544,8 +616,7 @@
 
     def cross(at):
         stage, rows = at[0], place_rows(at)
-        if at[1] == 0:
-            half_copy(stage, 0).wait_recv()
+        half_arrival(stage, 0)
         down_pair[stage, rows] = (
             down_share[stage, 2, rows].astype(F32) + down_in[stage, 0, rows].astype(F32)
         ).astype(BF16)
@@ -563,8 +634,7 @@
 
     def finish(at):
         stage, rows = at[0], place_rows(at)
-        if at[1] == 0:
-            half_copy(stage, 1).wait_recv()
+        half_arrival(stage, 1)
         cross_copy(at).wait_recv()
         finished[stage, rows] = (
             down_share[stage, 3, rows].astype(F32)
@@ -586,63 +656,52 @@
             select[source][:, 0:capacity], block, preferred_element_type=F32
         )
 
-    def each(action, stage, place):
-        if 0 <= stage < stages:
-            action((stage, place))
-
-    def each_remote(action, stage, place):
-        if (stage, place) != own:
-            each(action, stage, place)
-
-    each_remote(direct, 0, 1)
-    relay(own)
-    direct((0, 0))
-    each_remote(direct, 1, 1)
-    for copy in local[1:]:
-        copy.wait()
-    for stage in range(stages):
-        each_remote(relay, stage, 1)
-        if stage == stages - 1:
-            for early in range(stages - 2):
-                cross((early, 1))
-        expert_near(stage)
-        relay((stage, 0))
-        each(direct, stage + 1, 0)
-        each(cross, stage - 1, 0)
-        each_remote(direct, stage + 2, 1)
-        each(finish, stage - 2, 0)
-        expert_far(stage)
-    for stage in range(stages - 2):
-        finish((stage, 1))
-    cross((stages - 1, 0))
-    finish((stages - 2, 0))
-    cross((stages - 2, 1))
-    cross(own)
-    add_result((0, 0))
-    finish((stages - 1, 0))
-    add_result((0, 1))
-    finish((stages - 2, 1))
-    for stage in range(1, stages - 1):
-        add_result((stage, 0))
-        add_result((stage, 1))
-    finish(own)
-    add_result(own)
-    add_result((stages - 1, 0))
+    send_scales()
+    def send_later(at):
+        for k in range(2):
+            fill_rows(at, k)
+            send_rows(at, k)
+
+    def weights_here():
+        for copy in local[1:]:
+            copy.wait()
+
+    def sends_done():
+        for copy in halo_copies + to_partner + pair_copies + edge_copies + square_copies:
+            copy.wait_send()
+        for at in everyone:
+            if at != own:
+                row_copy(at, 0).wait_send()
+                row_copy(at, 1).wait_send()
+                scale_copy(at).wait_send()
+            for kind in range(3):
+                spread(at, kind).wait_send()
+            cross_copy(at).wait_send()
+        for stage in range(stages):
+            half_copy(stage, 0).wait_send()
+            half_copy(stage, 1).wait_send()
+
+    on_blocks = {"S": send_later, "D": direct, "L": relay, "X": cross, "F": finish, "A": add_result}
+    on_stages = {
+        "N": expert_near,
+        "G": expert_far,
+        "Q": lambda stage: [expert_down(stage, k) for k in (0, 1)],
+        "R": lambda stage: [expert_down(stage, k) for k in (2, 3)],
+    }
+    for step in plan_order(stages):
+        if step == "W":
+            weights_here()
+        elif step == "E":
+            sends_done()
+        elif step[0] in on_stages:
+            on_stages[step[0]](int(step[1]))
+        else:
+            on_blocks[step[0]]((int(step[1]), int(step[2])))
     out_ref[...] = stream[...].astype(BF16)
 
-    for copy in halo_copies + to_partner + pair_copies + edge_copies + square_copies:
-        copy.wait_send()
     for at in everyone:
         if at != own:
-            row_copy(at).wait_send()
-            scale_copy(at).wait_send()
             back_copy(at).wait_send()
-        for kind in range(3):
-            spread(at, kind).wait_send()
-        cross_copy(at).wait_send()
-    for stage in range(stages):
-        half_copy(stage, 0).wait_send()
-        half_copy(stage, 1).wait_send()
 
 
 def fused(
@@ -689,10 +748,10 @@
             pltpu.VMEM((1, tokens), jnp.int32),
             pltpu.VMEM((2, tokens, width), BF16),
             pltpu.VMEM((2, tokens, width), BF16),
-            pltpu.VMEM((tokens, width), BF16),
-            pltpu.VMEM((tokens, width), BF16),
-            pltpu.VMEM((3, 16, width), BF16),
-            pltpu.VMEM((3, 16, width), BF16),
+            pltpu.VMEM((2, tokens, width // 2), BF16),
+            pltpu.VMEM((2, tokens, width // 2), BF16),
+            pltpu.VMEM((2, 16, width), BF16),
+            pltpu.VMEM((2, 16, width), BF16),
             pltpu.VMEM((8, tokens), F32),
             pltpu.VMEM((3, 8, tokens), F32),
             pltpu.VMEM((sp_count, tokens), F32),
@@ -701,10 +760,11 @@
             pltpu.VMEM((sp_count, 8, slot_lanes), F32),
             pltpu.VMEM((sp_count, 8, slot_lanes), F32),
             pltpu.VMEM((tokens, width), F32),
-            pltpu.VMEM((sp_count, capacity, width), BF16),
-            pltpu.VMEM((stages, pair_rows, model_width), BF16),
+            pltpu.VMEM((sp_count, 2, capacity, width // 2), BF16),
+            pltpu.VMEM((stages, 4, 2, pair_rows, width // 2), BF16),
             pltpu.VMEM((2, hidden, pair_rows), F32),
             pltpu.VMEM((2, hidden, pair_rows), F32),
+            pltpu.VMEM((2, pair_rows, hidden), BF16),
             pltpu.VMEM((stages, 4, pair_rows, width), BF16),
             pltpu.VMEM((stages, 2, pair_rows, width), BF16),
             pltpu.VMEM((stages, pair_rows, width), BF16),
@@ -716,16 +776,16 @@
             dma((4,)),
             dma((3,)),
             dma((3,)),
+            dma((4,)),
+            dma((4,)),
             dma((2,)),
             dma((2,)),
             dma((3,)),
             dma((3,)),
-            dma((3,)),
-            dma((3,)),
             dma((sp_count,)),
             dma((sp_count,)),
-            dma((sp_count,)),
-            dma((sp_count,)),
+            dma((sp_count, 2)),
+            dma((sp_count, 2)),
             dma((sp_count, 3)),
             dma((sp_count, 3)),
             dma((stages, 2)),

time: 71.4 us -> 64.3 us (0.901)
  Pallas kernels: 69.6 us -> 62.5 us
    pallas_call x1, Pallas kernels: 69.6 us -> 62.5 us  [fused(): pl.pallas_call(functools.partial(layer_kernel, sp_count, capacity), out_s...]
where the time goes in v2:
time: 64.3 us; the launch traced here: 64.2 us
  Pallas kernels  62.5 us (97%)
  local copies, waits for them, and re-layouts  1.67 us (3%)
    pallas_call x1, Pallas kernels, fused(): pl.pallas_call(functools.partial(layer_kernel, sp_count, capacity), out_s...  62.5 us
    unnamed x1, local copies, waits for them, and re-layouts  1.67 us

profile of v2, /device:TPU:0, one launch (start us, length us, event | category | flops | bytes accessed | tf_op | source)
XLA Modules:
  0.0 64.2 jit_solution(4133518521085738936)
XLA Ops:
  0.0 62.5 %shard_map.127 = bf16[256,512]{1,0:T(8,128)(2,1)} custom-call(bf16[256,256]{1,0:T(8,128)(2,1)} %in_gate_ref.1, bf16[256,256]{1,0:T(8,128)(2,1)} %out_gate_ref.1, bf16[256,256]{1,0:T(8,128)(2,1)} %values_ref.1, bf16[3,256]{1,0:T(4,128)(2,1)} %taps_ref.1, s32[1,256]{1,0:T(1,128)} %bitcast.11, bf16[256,2048]{1,0:T(8,128)(2,1)} %residual_ref.1, ...), custom_call_target="tpu_custom_call" | custom-call | tf_op jit(solution)/shard_map/pallas_call | solution.py:734
  62.5 1.7 %copy.15 = bf16[256,512]{1,0:T(8,128)(2,1)} copy(bf16[256,512]{1,0:T(8,128)(2,1)} %shard_map.127) | data formatting | bytes 524288

commit v3 on v2

--- a/solution.py
+++ b/solution.py
@@ -126,7 +126,11 @@
 
 
 def plan_stages(planes):
-    far = [(mask, flip) for mask in range(planes // 2, planes) for flip in (0, 1)]
+    far = [
+        (mask, (flip + mask // (planes - 1)) % 2)
+        for mask in range(planes // 2, planes)
+        for flip in (0, 1)
+    ]
     near = [(0, 1)] + [(mask, flip) for mask in range(1, planes // 2) for flip in (0, 1)] + [(0, 0)]
     return list(zip(far, near))
 
@@ -141,13 +145,13 @@
     "Q1 R1 D30 X10",
     "N2 L20 X01 N3",
     "F00 G2 L30 Q2",
-    "R2 X20 X21 F10",
+    "R2 X20 X11 F10",
     "G3 Q3 R3 F01",
-    "X30 X11 X31 F20",
-    "A00 F21 F30 F11",
+    "X30 X21 X31 F20",
+    "A00 F11 F30 F21",
     "A10 A01 F31 A31",
-    "A20 A21 E A11",
-    "A30",
+    "A20 A11 E A30",
+    "A21",
 )
 
 

time: 64.3 us -> 65 us (1.011)
  Pallas kernels: 62.5 us -> 63.2 us
    pallas_call x1, Pallas kernels: 62.5 us -> 63.2 us  [fused(): pl.pallas_call(functools.partial(layer_kernel, sp_count, capacity), out_s...]
where the time goes in v3:
time: 65 us; the launch traced here: 64.8 us
  Pallas kernels  63.2 us (97%)
  local copies, waits for them, and re-layouts  1.67 us (3%)
    pallas_call x1, Pallas kernels, fused(): pl.pallas_call(functools.partial(layer_kernel, sp_count, capacity), out_s...  63.2 us
    unnamed x1, local copies, waits for them, and re-layouts  1.67 us

profile of v3, /device:TPU:0, one launch (start us, length us, event | category | flops | bytes accessed | tf_op | source)
XLA Modules:
  0.0 64.8 jit_solution(10968447164377084387)
XLA Ops:
  0.0 63.2 %shard_map.127 = bf16[256,512]{1,0:T(8,128)(2,1)} custom-call(bf16[256,256]{1,0:T(8,128)(2,1)} %in_gate_ref.1, bf16[256,256]{1,0:T(8,128)(2,1)} %out_gate_ref.1, bf16[256,256]{1,0:T(8,128)(2,1)} %values_ref.1, bf16[3,256]{1,0:T(4,128)(2,1)} %taps_ref.1, s32[1,256]{1,0:T(1,128)} %bitcast.11, bf16[256,2048]{1,0:T(8,128)(2,1)} %residual_ref.1, ...), custom_call_target="tpu_custom_call" | custom-call | tf_op jit(solution)/shard_map/pallas_call | solution.py:738
  63.2 1.7 %copy.15 = bf16[256,512]{1,0:T(8,128)(2,1)} copy(bf16[256,512]{1,0:T(8,128)(2,1)} %shard_map.127) | data formatting | bytes 524288
